TPU v7x, 32 devices: a whole 2x2x4 slice. The times are simulated.
32 devices in a mesh: fs: 4 (over z), tp: 8 (over y, x, core).
Axes of the slice: x: 2, y: 2, z: 4, core: 2. Of those that a mesh axis runs over, the one named last changes fastest.
Arguments:
- tokens: bfloat16 [768, 2304], P('fs'), may hold values from -6 to 6
- gate_train: float32 [8, 2304, 2304], P(None, 'fs', 'tp'), may hold values from -0.125 to 0.125
- up_train: float32 [8, 2304, 2304], P(None, 'fs', 'tp'), may hold values from -0.125 to 0.125
- down_train: float32 [8, 2304, 2304], P(None, 'fs', 'tp'), may hold values from -0.125 to 0.125
- gain: float32 [2304], P('fs'), may hold values from 0.1 to 1.9
- routes: int32 [768, 2], P('fs'), may hold values from 0 to 7, all different within a row; in each aligned block of 192 rows (0 to 191, 192 to 383, ...) at most 72 rows name the same one
- route_weights: float32 [768, 2], P('fs'), may hold values from 0.1 to 1
Outputs:
- gate_new: bfloat16 [8, 2304, 2304], P('tp')
- up_new: bfloat16 [8, 2304, 2304], P('tp')
- down_new: bfloat16 [8, 2304, 2304], P('tp')
- mixed: bfloat16 [768, 2304], P('fs', 'tp')
Inputs may be any that keep to these rules, and one draw needn't show every extreme that they name: `routes`: each row names two different experts; in each aligned block of 192 rows at most 72 rows name one expert, a bound that some block reaches.
All inputs are finite; a program needn't handle non-finite values.
Results may differ from a plain program's by a relative error of at most 0.0095.
Values may be sent and summed in bfloat16 or wider, within the bound.
A program may use at most 128 MiB of HBM per device.

v0:
```python
import jax
import jax.numpy as jnp
from jax import lax
from jax.sharding import PartitionSpec as P

CAP = 72
norm_eps = 1e-06


def arrange(matrix, tp_count):
    experts, row_count, col_count = matrix.shape
    slices = tp_count // experts
    piece_width = col_count // slices
    shaped = matrix.reshape(experts, row_count, slices, piece_width)
    return shaped.transpose(0, 2, 3, 1).reshape(tp_count, piece_width, row_count)


def shards(tokens, gate_train, up_train, down_train, gain, routes, route_weights):
    tp_count = lax.axis_size("tp")
    experts = gate_train.shape[0]
    slices = tp_count // experts
    gain_column = gain[None, :, None]
    gate_round = (gate_train * gain_column).astype(jnp.bfloat16)
    up_round = (up_train * gain_column).astype(jnp.bfloat16)
    down_round = down_train.astype(jnp.bfloat16)
    moved = (
        lax.all_to_all(
            arrange(gate_round, tp_count), "tp", split_axis=0, concat_axis=1, tiled=True
        ),
        lax.all_to_all(arrange(up_round, tp_count), "tp", split_axis=0, concat_axis=1, tiled=True),
        lax.all_to_all(
            arrange(down_round, tp_count), "tp", split_axis=0, concat_axis=1, tiled=True
        ),
    )
    tokens_wide = tokens.astype(jnp.float32)
    normed = (
        tokens_wide
        * lax.rsqrt(jnp.mean(tokens_wide * tokens_wide, axis=1, keepdims=True) + norm_eps)
    ).astype(jnp.bfloat16)
    expert = lax.axis_index("tp") // slices
    matches = routes == expert
    member = jnp.any(matches, axis=1)
    slot_index = jnp.cumsum(member.astype(jnp.int32)) - 1
    marked = jnp.where(member, slot_index, -1)
    picker = (marked[None, :] == jnp.arange(CAP, dtype=jnp.int32)[:, None]).astype(jnp.bfloat16)
    chosen = jnp.dot(picker, normed, preferred_element_type=jnp.float32).astype(jnp.bfloat16)
    contract_last = (((1,), (1,)), ((), ()))
    gate_new, up_new, down_new = (
        lax.all_gather(moved[0], "fs", axis=2, tiled=True),
        lax.all_gather(moved[1], "fs", axis=2, tiled=True),
        lax.all_gather(moved[2], "fs", axis=2, tiled=True),
    )
    gate_pre = lax.dot_general(
        chosen, gate_new[0], contract_last, preferred_element_type=jnp.float32
    )
    up_pre = lax.dot_general(chosen, up_new[0], contract_last, preferred_element_type=jnp.float32)
    hidden = (jax.nn.silu(gate_pre) * up_pre).astype(jnp.bfloat16)
    partial_value = jnp.dot(hidden, down_new[0], preferred_element_type=jnp.float32).astype(
        jnp.bfloat16
    )
    labels = jnp.arange(experts, dtype=jnp.int32)
    member_all = jnp.any(routes[:, :, None] == labels[None, None, :], axis=1)
    slots_all = jnp.cumsum(member_all.astype(jnp.int32), axis=0) - 1
    slot_pair = jnp.take_along_axis(slots_all, routes, axis=1)
    flat_index = slot_pair * experts + routes
    received = lax.all_to_all(
        partial_value.reshape(CAP, tp_count, -1), "tp", split_axis=1, concat_axis=1, tiled=True
    )
    summed = jnp.sum(received.reshape(CAP, experts, slices, -1).astype(jnp.float32), axis=2)
    summed = summed.reshape(CAP * experts, -1)
    picked = jnp.take(summed, flat_index, axis=0)
    mixed = jnp.sum(route_weights[:, :, None] * picked, axis=1)
    return (gate_new, up_new, down_new, mixed.astype(jnp.bfloat16))


def solution(mesh):
    in_specs = (
        P("fs", None),
        P(None, "fs", "tp"),
        P(None, "fs", "tp"),
        P(None, "fs", "tp"),
        P("fs"),
        P("fs", None),
        P("fs", None),
    )
    out_specs = (P("tp", None, None), P("tp", None, None), P("tp", None, None), P("fs", "tp"))
    return jax.shard_map(shards, mesh=mesh, in_specs=in_specs, out_specs=out_specs, check_vma=False)
```

profile of v0, /device:TPU:1, one launch (start us, length us, event | category | flops | bytes accessed | tf_op | source)
XLA Modules:
  0.0 690.3 jit_solution(4470130244694976679)
XLA Ops:
  7.2 5.4 fusion.16
  12.6 40.1 %all_to_all.41 = bf16[8,288,576]{2,1,0:T(8,128)(2,1)} all-to-all(bf16[8,288,576]{2,1,0:T(8,128)(2,1)S(1)} %get-tuple-element.23), channel_id=1, replica_groups=mesh['fs'=4,'tp'=8] {'tp'}, dimensions={0} | all-to-all | bytes 5308416 | tf_op jit(solution)/shard_map/all_to_all | solution.py:27
  52.6 4.5 copy.89
  57.2 39.1 %all_to_all.42 = bf16[8,288,576]{2,1,0:T(8,128)(2,1)} all-to-all(bf16[8,288,576]{2,1,0:T(8,128)(2,1)S(1)} %get-tuple-element.22), channel_id=1, replica_groups=mesh['fs'=4,'tp'=8] {'tp'}, dimensions={0} | all-to-all | bytes 5308416 | tf_op jit(solution)/shard_map/all_to_all | solution.py:30
  96.3 4.5 copy.90
  100.9 3.0 convert_bitcast_fusion
  103.9 38.2 %all_to_all.43 = bf16[8,288,576]{2,1,0:T(8,128)(2,1)S(1)} all-to-all(bf16[8,288,576]{2,1,0:T(8,128)(2,1)S(1)} %convert_bitcast_fusion), channel_id=1, replica_groups=mesh['fs'=4,'tp'=8] {'tp'}, dimensions={0} | all-to-all | bytes 5308416 | tf_op jit(solution)/shard_map/all_to_all | solution.py:31
  142.2 3.4 copy.91
  145.6 0.6 reduce-window.15
  146.8 2.7 gather_fusion.1
  150.6 0.4 convolution_convert_fusion
  151.0 91.9 %all-gather.4.cloned.1.call-done = bf16[1,2304,2304]{1,2,0:T(8,128)(2,1)} async-done(((bf16[1,2304,576]{1,2,0:T(8,128)(2,1)}), bf16[1,2304,2304]{1,2,0:T(8,128)(2,1)}) %all-gather.4.cloned.1.call-update) | async-done | bytes 10616848 | tf_op jit(solution)/shard_map/all_gather | solution.py:49
  242.9 6.0 fusion.4
  249.0 180.4 %all-gather.6.cloned.1.call-done = bf16[1,2304,2304]{1,2,0:T(8,128)(2,1)} async-done(((bf16[1,2304,576]{1,2,0:T(8,128)(2,1)}), bf16[1,2304,2304]{1,2,0:T(8,128)(2,1)}) %all-gather.6.cloned.1.call-update) | async-done | bytes 10616848 | tf_op jit(solution)/shard_map/all_gather | solution.py:50
  429.4 186.4 %all-gather.8.cloned.1.call-done = bf16[1,2304,2304]{1,2,0:T(8,128)(2,1)} async-done(((bf16[1,2304,576]{1,2,0:T(8,128)(2,1)}), bf16[1,2304,2304]{1,2,0:T(8,128)(2,1)}) %all-gather.8.cloned.1.call-update) | async-done | bytes 10616848 | tf_op jit(solution)/shard_map/all_gather | solution.py:51
  615.8 11.9 %fusion.12 = bf16[72,2304]{1,0:T(8,128)(2,1)S(1)} fusion(bf16[1,2304,2304]{1,2,0:T(8,128)(2,1)} %all-gather.8.cloned.1.call-done, bf16[72,2304]{1,0:T(8,128)(2,1)S(1)} %convolution_convert_fusion, bf16[1,2304,2304]{1,2,0:T(8,128)(2,1)} %all-gather.6.cloned.1.call-done, f32[72,2304]{1,0:T(8,128)S(1)} %fusion.4), kind=kOutput, calls=%fused_computation.12 | convolution fusion | flops 1529985024 | bytes 22560768 | tf_op jit(solution)/shard_map/dot_general | solution.py:58
  627.7 0.7 reshape.112
  628.4 0.8 copy.96
  629.2 4.2 all-to-all-start.3
  633.9 15.2 %copy.100 = bf16[1,2304,2304]{2,1,0:T(8,128)(2,1)} copy(bf16[1,2304,2304]{1,2,0:T(8,128)(2,1)} %all-gather.6.cloned.1.call-done) | data formatting | bytes 21233664
  649.1 15.2 %copy.99 = bf16[1,2304,2304]{2,1,0:T(8,128)(2,1)} copy(bf16[1,2304,2304]{1,2,0:T(8,128)(2,1)} %all-gather.4.cloned.1.call-done) | data formatting | bytes 21233664
  664.4 15.2 %copy.101 = bf16[1,2304,2304]{2,1,0:T(8,128)(2,1)} copy(bf16[1,2304,2304]{1,2,0:T(8,128)(2,1)} %all-gather.8.cloned.1.call-done) | data formatting | bytes 21233664
  679.6 1.7 gather_fusion
  681.7 2.0 multiply_reduce_fusion
  (42 shorter events, 2.9 us)
Async XLA Ops:
  7.2 235.8 %all-gather.4.cloned.1.call-start = ((), (), s32[]{:S(2)}) async-start(), calls=%async_computation.4 | async-start | bytes 13271040 | tf_op jit(solution)/shard_map/all_gather | solution.py:49
  57.1 372.2 %all-gather.6.cloned.1.call-start = ((), (), s32[]{:S(2)}) async-start(), calls=%async_computation.5 | async-start | bytes 13271040 | tf_op jit(solution)/shard_map/all_gather | solution.py:50
  100.8 514.9 %all-gather.8.cloned.1.call-start = ((), (), s32[]{:S(2)}) async-start(), calls=%async_computation.6 | async-start | bytes 13271040 | tf_op jit(solution)/shard_map/all_gather | solution.py:51
  103.9 41.7 %copy-start.1 = (s32[192,2]{0,1:T(2,128)S(1)}, s32[192,2]{0,1:T(2,128)}, u32[]{:S(2)}) copy-start(s32[192,2]{0,1:T(2,128)} %param.12) | copy-start | bytes 4612
  146.8 3.5 copy-start
  248.9 384.8 %copy-start.2 = (f32[192,2]{0,1:T(2,128)S(1)}, f32[192,2]{0,1:T(2,128)}, u32[]{:S(2)}) copy-start(f32[192,2]{0,1:T(2,128)} %param.13) | copy-start | bytes 4612
  629.2 50.4 %all-to-all-start.3 = ((bf16[72,8,288]{2,0,1:T(8,128)(2,1)}), bf16[72,8,288]{2,0,1:T(8,128)(2,1)S(1)}, u32[]{:S(2)}, u32[]{:S(2)}) async-start(bf16[72,8,288]{2,0,1:T(8,128)(2,1)} %copy.96), calls=%async_computation.3 | async-start | bytes 884736 | tf_op jit(solution)/shard_map/all_to_all | solution.py:66
Sparse Core Ops, SparseCore 0:
  57.3 185.6 all-gather.3
  245.1 184.2 all-gather.5
  431.5 184.2 all-gather.7
where the time goes:
time: 692 us; the launch traced here: 690 us
  waiting for transfers between devices  459 us (66%)
  blocking collectives  117 us (17%)
  local copies, waits for them, and re-layouts  65.7 us (9%)
  matrix products  18.3 us (3%)
  between operations  13.9 us (2%)
  other arithmetic  11.9 us (2%)
    all_gather x1, waiting for transfers between devices, shards(): lax.all_gather(moved[2], 'fs', axis=2, tiled=True)  186 us
    all_gather x1, waiting for transfers between devices, shards(): lax.all_gather(moved[1], 'fs', axis=2, tiled=True)  180 us
    all_gather x1, waiting for transfers between devices, shards(): lax.all_gather(moved[0], 'fs', axis=2, tiled=True)  91.9 us
    unnamed x10, local copies, waits for them, and re-layouts  45.8 us
    all_to_all x1, blocking collectives, shards(): lax.all_to_all(arrange(gate_round, tp_count), 'tp', split_axis=0, concat_...  40.1 us
    all_to_all x1, blocking collectives, shards(): lax.all_to_all(arrange(up_round, tp_count), 'tp', split_axis=0, concat_ax...  39.1 us
    all_to_all x1, blocking collectives, shards(): lax.all_to_all(arrange(down_round, tp_count), 'tp', split_axis=0, concat_...  38.2 us
  transfers between devices with their start and end apart: 4, of which 3 were waited for; matrix products, arithmetic and copies ran while one was open for 10% of the time, Pallas kernels for 0%

commit v1 on v0

--- a/solution.py
+++ b/solution.py
@@ -1,3 +1,4 @@
+import functools
 import jax
 import jax.numpy as jnp
 from jax import lax
@@ -5,6 +6,15 @@
 
 CAP = 72
 norm_eps = 1e-06
+
+
+def number_numbers_all(inputs, axis_id):
+    upper = lax.all_gather(inputs, axis_id)
+    val = jnp.concatenate(upper, 2)
+    return val
+
+
+drive_the_axis_part = functools.partial(number_numbers_all, axis_id="fs")
 
 
 def arrange(matrix, tp_count):
@@ -47,7 +57,7 @@
     contract_last = (((1,), (1,)), ((), ()))
     gate_new, up_new, down_new = (
         lax.all_gather(moved[0], "fs", axis=2, tiled=True),
-        lax.all_gather(moved[1], "fs", axis=2, tiled=True),
+        drive_the_axis_part(moved[1]),
         lax.all_gather(moved[2], "fs", axis=2, tiled=True),
     )
     gate_pre = lax.dot_general(

time: 692 us -> 692 us (level)
  no operation moved by 1% of the time
where the time goes in v1:
time: 692 us; the launch traced here: 690 us
  waiting for transfers between devices  459 us (66%)
  blocking collectives  117 us (17%)
  local copies, waits for them, and re-layouts  65.7 us (9%)
  matrix products  18.3 us (3%)
  between operations  13.9 us (2%)
  other arithmetic  11.9 us (2%)
    all_gather x1, waiting for transfers between devices, shards(): lax.all_gather(moved[2], 'fs', axis=2, tiled=True)  186 us
    all_gather x1, waiting for transfers between devices, number_numbers_all(): upper = lax.all_gather(inputs, axis_id)  180 us
    all_gather x1, waiting for transfers between devices, shards(): lax.all_gather(moved[0], 'fs', axis=2, tiled=True)  91.9 us
    unnamed x10, local copies, waits for them, and re-layouts  45.8 us
    all_to_all x1, blocking collectives, shards(): lax.all_to_all(arrange(gate_round, tp_count), 'tp', split_axis=0, concat_...  40.1 us
    all_to_all x1, blocking collectives, shards(): lax.all_to_all(arrange(up_round, tp_count), 'tp', split_axis=0, concat_ax...  39.1 us
    all_to_all x1, blocking collectives, shards(): lax.all_to_all(arrange(down_round, tp_count), 'tp', split_axis=0, concat_...  38.2 us
  transfers between devices with their start and end apart: 4, of which 3 were waited for; matrix products, arithmetic and copies ran while one was open for 10% of the time, Pallas kernels for 0%

profile of v1, /device:TPU:1, one launch (start us, length us, event | category | flops | bytes accessed | tf_op | source)
XLA Modules:
  0.0 690.3 jit_solution(16407702111998568048)
XLA Ops:
  7.2 5.4 fusion.9
  12.6 40.1 %all_to_all.38 = bf16[8,288,576]{2,1,0:T(8,128)(2,1)} all-to-all(bf16[8,288,576]{2,1,0:T(8,128)(2,1)S(1)} %get-tuple-element.31), channel_id=1, replica_groups=mesh['fs'=4,'tp'=8] {'tp'}, dimensions={0} | all-to-all | bytes 5308416 | tf_op jit(solution)/shard_map/all_to_all | solution.py:37
  52.6 4.5 copy.111
  57.2 39.1 %all_to_all.39 = bf16[8,288,576]{2,1,0:T(8,128)(2,1)} all-to-all(bf16[8,288,576]{2,1,0:T(8,128)(2,1)S(1)} %get-tuple-element.30), channel_id=1, replica_groups=mesh['fs'=4,'tp'=8] {'tp'}, dimensions={0} | all-to-all | bytes 5308416 | tf_op jit(solution)/shard_map/all_to_all | solution.py:40
  96.3 4.5 copy.112
  100.9 3.0 convert_bitcast_fusion
  103.9 38.2 %all_to_all.40 = bf16[8,288,576]{2,1,0:T(8,128)(2,1)S(1)} all-to-all(bf16[8,288,576]{2,1,0:T(8,128)(2,1)S(1)} %convert_bitcast_fusion), channel_id=1, replica_groups=mesh['fs'=4,'tp'=8] {'tp'}, dimensions={0} | all-to-all | bytes 5308416 | tf_op jit(solution)/shard_map/all_to_all | solution.py:41
  142.2 3.4 copy.114
  145.6 0.6 reduce-window.15
  146.8 2.7 gather_fusion.1
  150.6 0.4 convolution_convert_fusion
  151.0 91.9 %all-gather.4.cloned.1.call-done = bf16[1,2304,2304]{1,2,0:T(8,128)(2,1)} async-done(((bf16[1,2304,576]{1,2,0:T(8,128)(2,1)}), bf16[1,2304,2304]{1,2,0:T(8,128)(2,1)}) %all-gather.4.cloned.1.call-update) | async-done | bytes 10616848 | tf_op jit(solution)/shard_map/all_gather | solution.py:59
  242.9 6.0 fusion.2
  248.9 180.4 %all-gather.6.cloned.1.call-done = bf16[4,1,2304,576]{2,3,1,0:T(8,128)(2,1)} async-done(((bf16[1,1,2304,576]{2,3,1,0:T(8,128)(2,1)}), bf16[4,1,2304,576]{2,3,1,0:T(8,128)(2,1)}) %all-gather.6.cloned.1.call-update) | async-done | bytes 10616848 | tf_op jit(solution)/shard_map/all_gather | solution.py:12
  429.4 186.4 %all-gather.8.cloned.1.call-done = bf16[1,2304,2304]{1,2,0:T(8,128)(2,1)} async-done(((bf16[1,2304,576]{1,2,0:T(8,128)(2,1)}), bf16[1,2304,2304]{1,2,0:T(8,128)(2,1)}) %all-gather.8.cloned.1.call-update) | async-done | bytes 10616848 | tf_op jit(solution)/shard_map/all_gather | solution.py:61
  615.8 11.9 %fusion.5 = bf16[72,2304]{1,0:T(8,128)(2,1)S(1)} fusion(bf16[1,2304,2304]{1,2,0:T(8,128)(2,1)} %all-gather.8.cloned.1.call-done, bf16[72,2304]{1,0:T(8,128)(2,1)S(1)} %convolution_convert_fusion, bf16[2304,2304]{0,1:T(8,128)(2,1)} %bitcast.57, f32[72,2304]{1,0:T(8,128)S(1)} %fusion.2), kind=kOutput, calls=%fused_computation.10 | convolution fusion | flops 1529985024 | bytes 22560768 | tf_op jit(solution)/shard_map/dot_general | solution.py:68
  627.7 0.7 reshape.121
  628.4 0.8 copy.119
  629.2 4.2 all-to-all-start.3
  633.9 15.2 %copy.123 = bf16[1,2304,2304]{2,1,0:T(8,128)(2,1)} copy(bf16[1,2304,2304]{1,2,0:T(8,128)(2,1)} %bitcast.58) | data formatting | bytes 21233664
  649.2 15.2 %copy.122 = bf16[1,2304,2304]{2,1,0:T(8,128)(2,1)} copy(bf16[1,2304,2304]{1,2,0:T(8,128)(2,1)} %all-gather.4.cloned.1.call-done) | data formatting | bytes 21233664
  664.4 15.2 %copy.124 = bf16[1,2304,2304]{2,1,0:T(8,128)(2,1)} copy(bf16[1,2304,2304]{1,2,0:T(8,128)(2,1)} %all-gather.8.cloned.1.call-done) | data formatting | bytes 21233664
  679.6 1.7 gather_fusion
  681.7 2.0 multiply_reduce_fusion
  (42 shorter events, 2.9 us)
Async XLA Ops:
  7.2 235.8 %all-gather.4.cloned.1.call-start = ((), (), s32[]{:S(2)}) async-start(), calls=%async_computation.4 | async-start | bytes 13271040 | tf_op jit(solution)/shard_map/all_gather | solution.py:59
  57.1 372.2 %all-gather.6.cloned.1.call-start = ((), (), s32[]{:S(2)}) async-start(), calls=%async_computation.5 | async-start | bytes 13271040 | tf_op jit(solution)/shard_map/all_gather | solution.py:12
  100.8 514.9 %all-gather.8.cloned.1.call-start = ((), (), s32[]{:S(2)}) async-start(), calls=%async_computation.6 | async-start | bytes 13271040 | tf_op jit(solution)/shard_map/all_gather | solution.py:61
  103.9 41.7 %copy-start.1 = (s32[192,2]{0,1:T(2,128)S(1)}, s32[192,2]{0,1:T(2,128)}, u32[]{:S(2)}) copy-start(s32[192,2]{0,1:T(2,128)} %param.12) | copy-start | bytes 4612
  146.8 3.5 copy-start
  615.8 18.0 %copy-start.2 = (f32[192,2]{0,1:T(2,128)S(1)}, f32[192,2]{0,1:T(2,128)}, u32[]{:S(2)}) copy-start(f32[192,2]{0,1:T(2,128)} %param.13) | copy-start | bytes 4612
  629.2 50.4 %all-to-all-start.3 = ((bf16[72,8,288]{2,0,1:T(8,128)(2,1)}), bf16[72,8,288]{2,0,1:T(8,128)(2,1)S(1)}, u32[]{:S(2)}, u32[]{:S(2)}) async-start(bf16[72,8,288]{2,0,1:T(8,128)(2,1)} %copy.119), calls=%async_computation.3 | async-start | bytes 884736 | tf_op jit(solution)/shard_map/all_to_all | solution.py:76
Sparse Core Ops, SparseCore 0:
  57.3 185.6 all-gather.3
  245.1 184.2 all-gather.5
  431.5 184.2 all-gather.7
